TPU v7x, 32 devices: a whole 2x2x4 slice. The times are simulated.
32 devices in a mesh: kv: 16 (over z, y, x), tp: 2 (over core).
Axes of the slice: x: 2, y: 2, z: 4, core: 2. Of those that a mesh axis runs over, the one named last changes fastest.
Arguments:
- tokens: bfloat16 [160, 3, 2048], P('kv', None, 'tp'), may hold values from -6 to 6
- norm_gain: float32 [2048], replicated, may hold values from 0.1 to 1.9
- w_query: bfloat16 [2048, 1024], P('kv', 'tp'), may hold values from -0.125 to 0.125
- w_key: bfloat16 [2048, 1024], P('kv', 'tp'), may hold values from -0.125 to 0.125
- w_value: bfloat16 [2048, 2048], P('kv', 'tp'), may hold values from -0.125 to 0.125
- w_igate: bfloat16 [2048, 8], replicated, may hold values from -0.125 to 0.125
- w_fgate: bfloat16 [2048, 8], replicated, may hold values from -0.125 to 0.125
- igate_bias: float32 [8], replicated, may hold values from -5 to -2
- fgate_bias: float32 [8], replicated, may hold values from 0.5 to 4
- prev_keys: bfloat16 [160, 3, 1024], P('kv', None, 'tp'), may hold values from -6 to 6
- prev_values: bfloat16 [160, 3, 2048], P('kv', None, 'tp'), may hold values from -6 to 6
- prev_igate: float32 [160, 3, 8], P('kv', None, 'tp'), may hold values from -4 to 0
- prev_logf: float32 [160, 3, 8], P('kv', None, 'tp'), may hold values from -0.6 to -0.02
- accepted: int32 [160], P('kv'), may hold values from 0 to 3
- state_mem: float32 [160, 8, 128, 256], P('kv', 'tp'), may hold values from -2 to 2
- state_norm: float32 [160, 8, 128], P('kv', 'tp'), may hold values from -2 to 2
- state_max: float32 [160, 8], P('kv', 'tp'), may hold values from -3 to 0
Outputs:
- readout: bfloat16 [160, 3, 2048], P('kv', None, 'tp')
- base_mem: float32 [160, 8, 128, 256], P('kv', 'tp')
- base_norm: float32 [160, 8, 128], P('kv', 'tp')
- base_max: float32 [160, 8], P('kv', 'tp')
Inputs may be any that keep to these rules, and one draw needn't show every extreme that they name: Proposal j of a sequence is live when j < accepted of that sequence.
All inputs are finite; a program needn't handle non-finite values.
Results may differ from a plain program's by a relative error of at most 0.0073.
Values may be sent and summed in bfloat16 or wider, within the bound.
No kernel may reach another device: no remote copies, remote signals or barrier semaphores. Data moves between devices by JAX's collectives and lax.ppermute only.
A program may use at most 64 MiB of HBM per device.

v0:
```python
import jax
import jax.numpy as jnp
from jax import lax
from jax.sharding import PartitionSpec as P

epsilon = 1e-06
highest = lax.Precision.HIGHEST


def fold_accepted(
    state_mem, state_norm, state_max, key_rows, value_rows, in_gate, log_forget, accepted
):
    length = key_rows.shape[1]
    live_mask = (jnp.arange(length, dtype=jnp.int32)[None, :] < accepted[:, None])[:, :, None]
    forget_live = jnp.where(live_mask, log_forget, 0.0)
    cumulative = jnp.cumsum(forget_live, axis=1)
    totals = cumulative[:, -1]
    weight_log = jnp.where(live_mask, totals[:, None] - cumulative + in_gate, -jnp.inf)
    base_max = jnp.maximum(totals + state_max, jnp.max(weight_log, axis=1))
    carry_weight = jnp.exp(totals + state_max - base_max)
    weights = jnp.exp(weight_log - base_max[:, None])
    base_mem = carry_weight[..., None, None] * state_mem + jnp.einsum(
        "sph,sphd,sphv->shdv", weights, key_rows, value_rows, precision=highest
    )
    base_norm = carry_weight[..., None] * state_norm + jnp.einsum(
        "sph,sphd->shd", weights, key_rows, precision=highest
    )
    return (base_mem, base_norm, base_max)


def readout_block(
    base_mem, base_norm, base_max, query_rows, key_rows, value_rows, in_gate, log_forget
):
    length = query_rows.shape[1]
    cumulative = jnp.cumsum(log_forget, axis=1)
    causal = (
        jnp.arange(length, dtype=jnp.int32)[:, None] >= jnp.arange(length, dtype=jnp.int32)[None, :]
    )
    within_log = cumulative[:, :, None, :] - cumulative[:, None, :, :] + in_gate[:, None, :, :]
    within_log = jnp.where(causal[None, :, :, None], within_log, -jnp.inf)
    carried_log = cumulative + base_max[:, None, :]
    top_log = jnp.maximum(carried_log, jnp.max(within_log, axis=2))
    scores = jnp.einsum("sthd,suhd->stuh", query_rows, key_rows, precision=highest) * jnp.exp(
        within_log - top_log[:, :, None, :]
    )
    carried_weight = jnp.exp(carried_log - top_log)
    numerator = jnp.einsum(
        "stuh,suhv->sthv", scores, value_rows, precision=highest
    ) + carried_weight[..., None] * jnp.einsum(
        "sthd,shdv->sthv", query_rows, base_mem, precision=highest
    )
    denominator = jnp.sum(scores, axis=2) + carried_weight * jnp.einsum(
        "sthd,shd->sth", query_rows, base_norm, precision=highest
    )
    return numerator / jnp.maximum(jnp.abs(denominator), jnp.exp(-top_log))[..., None]


def shards(
    tokens,
    norm_gain,
    w_query,
    w_key,
    w_value,
    w_igate,
    w_fgate,
    igate_bias,
    fgate_bias,
    prev_keys,
    prev_values,
    prev_igate,
    prev_logf,
    accepted,
    state_mem,
    state_norm,
    state_max,
):
    seq_count, length, part_width = tokens.shape
    head_count = state_mem.shape[1]
    key_width = state_mem.shape[2]
    value_width = state_mem.shape[3]
    key_scale = key_width ** (-0.5)
    row_count = seq_count * length
    gathered = lax.all_gather(tokens.reshape(row_count, part_width), "tp", axis=1, tiled=True)
    flattened = gathered.astype(jnp.float32)
    normed = (
        flattened
        * lax.rsqrt(jnp.mean(flattened * flattened, axis=-1, keepdims=True) + epsilon)
        * norm_gain
    ).astype(jnp.bfloat16)
    stacked = jnp.concatenate([w_query, w_key, w_value], axis=1)
    spread = lax.all_to_all(normed, "kv", split_axis=1, concat_axis=0, tiled=True)
    projected = lax.psum_scatter(
        jnp.dot(spread, stacked, preferred_element_type=jnp.float32),
        "kv",
        scatter_dimension=0,
        tiled=True,
    )
    query_cols = head_count * key_width
    query_rows = projected[:, :query_cols].astype(jnp.bfloat16)
    key_rows = projected[:, query_cols : 2 * query_cols].astype(jnp.bfloat16)
    value_rows = projected[:, 2 * query_cols :].astype(jnp.bfloat16)
    head_start = lax.axis_index("tp") * head_count
    input_weight = lax.dynamic_slice_in_dim(w_igate, head_start, head_count, 1)
    forget_weight = lax.dynamic_slice_in_dim(w_fgate, head_start, head_count, 1)
    in_gate = jnp.dot(
        normed, input_weight, preferred_element_type=jnp.float32
    ) + lax.dynamic_slice_in_dim(igate_bias, head_start, head_count, 0)
    log_forget = jax.nn.log_sigmoid(
        jnp.dot(normed, forget_weight, preferred_element_type=jnp.float32)
        + lax.dynamic_slice_in_dim(fgate_bias, head_start, head_count, 0)
    )

    def split_heads(matrix, last_width):
        return matrix.astype(jnp.float32).reshape(seq_count, length, head_count, last_width)

    base_mem, base_norm, base_max = fold_accepted(
        state_mem,
        state_norm,
        state_max,
        split_heads(prev_keys, key_width) * key_scale,
        split_heads(prev_values, value_width),
        prev_igate,
        prev_logf,
        accepted,
    )
    hidden = readout_block(
        base_mem,
        base_norm,
        base_max,
        split_heads(query_rows, key_width),
        split_heads(key_rows, key_width) * key_scale,
        split_heads(value_rows, value_width),
        in_gate.reshape(seq_count, length, head_count),
        log_forget.reshape(seq_count, length, head_count),
    )
    readout = hidden.reshape(seq_count, length, head_count * value_width).astype(jnp.bfloat16)
    return (readout, base_mem, base_norm, base_max)


def solution(mesh):
    return jax.shard_map(
        shards,
        mesh=mesh,
        in_specs=(
            P("kv", None, "tp"),
            P(),
            P("kv", "tp"),
            P("kv", "tp"),
            P("kv", "tp"),
            P(),
            P(),
            P(),
            P(),
            P("kv", None, "tp"),
            P("kv", None, "tp"),
            P("kv", None, "tp"),
            P("kv", None, "tp"),
            P("kv"),
            P("kv", "tp", None, None),
            P("kv", "tp", None),
            P("kv", "tp"),
        ),
        out_specs=(
            P("kv", None, "tp"),
            P("kv", "tp", None, None),
            P("kv", "tp", None),
            P("kv", "tp"),
        ),
        check_vma=False,
    )
```

profile of v0, /device:TPU:16, one launch (start us, length us, event | category | flops | bytes accessed | tf_op | source)
XLA Modules:
  0.0 143.2 jit_solution(959274244908550986)
XLA Ops:
  0.6 0.0 copy-start
  0.6 1.0 reshape.103
  1.6 1.9 %all_gather.3 = bf16[30,2048]{1,0:T(8,128)(2,1)S(1)} all-gather(bf16[30,1024]{1,0:T(8,128)(2,1)S(1)} %reshape.103), channel_id=1, replica_groups=mesh['kv'=16,'tp'=2] {'tp'}, dimensions={1}, use_global_device_ids=true | all-gather | bytes 184320 | tf_op jit(solution)/shard_map/all_gather | solution.py:83
  3.5 0.1 fusion.13
  3.7 0.8 fusion.15
  4.5 0.7 copy.114
  5.2 7.1 %all-to-all-start = ((bf16[30,16,128]{2,0,1:T(8,128)(2,1)}), bf16[30,16,128]{2,0,1:T(8,128)(2,1)S(1)}, u32[]{:S(2)}, u32[]{:S(2)}) async-start(bf16[30,16,128]{2,0,1:T(8,128)(2,1)} %copy.114), calls=%async_computation | async-start | bytes 262144 | tf_op jit(solution)/shard_map/all_to_all | solution.py:91
  12.3 0.7 iota_compare_fusion
  13.0 0.7 dynamic_slice.15
  13.7 0.7 dynamic_slice.13
  14.4 0.7 fusion.31
  15.1 0.1 copy.121
  15.2 0.7 fusion.44
  15.9 0.1 copy.143
  16.0 0.8 copy.122
  16.8 0.1 copy.124
  16.9 0.0 copy-start.6
  16.9 0.8 reshape.111
  17.7 0.9 fusion.37
  18.7 0.1 reshape.106
  18.8 0.1 copy.117
  18.9 0.1 copy.118
  19.0 0.9 convolution_add_fusion
  19.9 0.1 add.89
  20.0 0.2 fusion.19
  20.2 0.1 copy.125
  20.3 0.1 copy.130
  20.4 0.1 broadcast_multiply_fusion
  20.5 0.0 copy-done
  20.6 0.0 copy-start.7
  20.6 0.0 copy-start.1
  20.6 0.0 copy-start.2
  20.6 0.0 copy-start.3
  20.6 8.0 %multiply_add_fusion = f32[10,4,128,256]{3,2,1,0:T(8,128)} fusion(f32[10,4,128,256]{3,2,1,0:T(8,128)} %param.31, f32[10,4]{1,0:T(8,128)S(1)} %get-tuple-element.14, bf16[10,3,4,256]{3,1,2,0:T(4,128)(2,1)S(1)} %bitcast.57, f32[10,3,4,128]{3,2,1,0:T(4,128)S(1)} %get-tuple-element.19), kind=kOutput, calls=%fused_computation | convolution fusion | flops 49807360 | bytes 10608800 | tf_op jit(solution)/shard_map/sph,sphd,sphv->shdv/dot_general | solution.py:22
  28.6 0.1 copy.138
  28.7 0.1 copy.126
  28.8 0.0 copy-done.7
  28.8 0.6 dynamic-slice.4
  30.0 0.4 fusion.20
  30.4 0.0 all-to-all-done
  30.5 0.0 copy-done.1
  30.5 0.0 copy-done.2
  30.5 0.0 copy-done.3
  30.5 0.0 copy-start.4
  30.5 2.5 %fusion.7 = f32[480,2048]{1,0:T(8,128)} fusion(bf16[480,128]{1,0:T(8,128)(2,1)S(1)} %all_to_all.17, bf16[128,1024]{1,0:T(8,128)(2,1)S(1)} %copy-done.1, bf16[128,512]{1,0:T(8,128)(2,1)S(1)} %copy-done.2, bf16[128,512]{1,0:T(8,128)(2,1)S(1)} %copy-done.3), kind=kOutput, calls=%fused_computation.12 | convolution fusion | flops 253231104 | bytes 4579328 | tf_op jit(solution)/shard_map/dot_general | solution.py:93
  33.1 94.6 %fusion = f32[32,2048]{1,0:T(8,128)S(1)} fusion(f32[480,2048]{1,0:T(8,128)} %fusion.7), kind=kCustom, calls=%all-reduce-scatter | all-reduce-scatter fusion | flops 1048577 | bytes 4194816
  127.8 1.9 %collective-permute-start = (bf16[30,2048]{1,0:T(8,128)(2,1)S(1)}, bf16[30,2048]{1,0:T(8,128)(2,1)S(1)}, u32[]{:S(2)}, u32[]{:S(2)}) collective-permute-start(bf16[30,2048]{1,0:T(8,128)(2,1)S(1)} %slice.23), channel_id=1, source_target_pairs={{0,2},{2,4},{4,6},{6,8},{8,10},{10,12},{12,14},{14,16},{16,18},{18... | collective-permute-start | bytes 368648
  129.7 0.0 copy-done.4
  129.7 0.1 multiply_add_fusion.1
  129.8 0.0 copy-start.5
  129.8 6.7 %collective-permute-done = bf16[30,2048]{1,0:T(8,128)(2,1)S(1)} collective-permute-done((bf16[30,2048]{1,0:T(8,128)(2,1)S(1)}, bf16[30,2048]{1,0:T(8,128)(2,1)S(1)}, u32[]{:S(2)}, u32[]{:S(2)}) %collective-permute-start) | collective-permute-done | bytes 122912
  136.5 0.3 concatenate.4
  136.8 0.3 fusion.23
  137.1 0.1 copy.142
  137.3 0.3 fusion.45
  137.6 0.1 copy.134
  137.7 0.0 copy-done.6
  137.8 0.1 copy.135
  137.9 0.1 copy.129
  138.0 4.2 %fusion.3 = f32[10,3,4,256]{3,1,2,0:T(4,128)S(1)} fusion(f32[10,4,128,256]{3,2,1,0:T(8,128)} %multiply_add_fusion, f32[10,3,4]{1,2,0:T(4,128)S(1)} %copy.129, bf16[10,3,4,128]{3,2,1,0:T(4,128)(2,1)S(1)} %reshape.105), kind=kOutput, calls=%fused_computation.5 | convolution fusion | flops 47216640 | bytes 5396960 | tf_op jit(solution)/shard_map/sthd,shdv->sthv/dot_general | solution.py:49
  142.2 1.0 fusion.4
  143.2 0.0 copy-done.5
  (19 shorter events, 0.3 us)
Async XLA Ops:
  0.6 19.9 %copy-start = (bf16[10,3,1024]{2,1,0:T(4,128)(2,1)S(1)}, bf16[10,3,1024]{2,1,0:T(4,128)(2,1)}, u32[]{:S(2)}) copy-start(bf16[10,3,1024]{2,1,0:T(4,128)(2,1)} %param.27) | copy-start | bytes 184324
  5.2 25.2 %all-to-all-start = ((bf16[30,16,128]{2,0,1:T(8,128)(2,1)}), bf16[30,16,128]{2,0,1:T(8,128)(2,1)S(1)}, u32[]{:S(2)}, u32[]{:S(2)}) async-start(bf16[30,16,128]{2,0,1:T(8,128)(2,1)} %copy.114), calls=%async_computation | async-start | bytes 262144 | tf_op jit(solution)/shard_map/all_to_all | solution.py:91
  16.9 120.8 %copy-start.6 = (f32[10,4]{0,1:T(4,128)}, f32[10,4]{0,1:T(4,128)S(1)}, u32[]{:S(2)}) copy-start(f32[10,4]{0,1:T(4,128)S(1)} %copy.124) | copy-start | bytes 484
  20.6 8.2 %copy-start.7 = (u32[32]{0:T(128)S(1)}, u32[32]{0:T(128)}, u32[]{:S(2)}) copy-start(u32[32]{0:T(128)} %constant.39) | copy-start | bytes 388
  20.6 9.9 %copy-start.1 = (bf16[128,1024]{1,0:T(8,128)(2,1)S(1)}, bf16[128,1024]{1,0:T(8,128)(2,1)}, u32[]{:S(2)}) copy-start(bf16[128,1024]{1,0:T(8,128)(2,1)} %param.21) | copy-start | bytes 786436
  20.6 9.9 %copy-start.2 = (bf16[128,512]{1,0:T(8,128)(2,1)S(1)}, bf16[128,512]{1,0:T(8,128)(2,1)}, u32[]{:S(2)}) copy-start(bf16[128,512]{1,0:T(8,128)(2,1)} %param.20) | copy-start | bytes 393220
  20.6 9.9 %copy-start.3 = (bf16[128,512]{1,0:T(8,128)(2,1)S(1)}, bf16[128,512]{1,0:T(8,128)(2,1)}, u32[]{:S(2)}) copy-start(bf16[128,512]{1,0:T(8,128)(2,1)} %param.19) | copy-start | bytes 393220
  30.5 99.2 %copy-start.4 = (f32[10,4,128]{2,1,0:T(4,128)S(1)}, f32[10,4,128]{2,1,0:T(4,128)}, u32[]{:S(2)}) copy-start(f32[10,4,128]{2,1,0:T(4,128)} %param.32) | copy-start | bytes 61444
  127.8 8.7 %collective-permute-start = (bf16[30,2048]{1,0:T(8,128)(2,1)S(1)}, bf16[30,2048]{1,0:T(8,128)(2,1)S(1)}, u32[]{:S(2)}, u32[]{:S(2)}) collective-permute-start(bf16[30,2048]{1,0:T(8,128)(2,1)S(1)} %slice.23), channel_id=1, source_target_pairs={{0,2},{2,4},{4,6},{6,8},{8,10},{10,12},{12,14},{14,16},{16,18},{18... | collective-permute-start | bytes 368648
  129.8 13.4 %copy-start.5 = (f32[10,4,128]{2,1,0:T(4,128)}, f32[10,4,128]{2,1,0:T(4,128)S(1)}, u32[]{:S(2)}) copy-start(f32[10,4,128]{2,1,0:T(4,128)S(1)} %multiply_add_fusion.1) | copy-start | bytes 61444
where the time goes:
time: 144 us; the launch traced here: 143 us
  blocking collectives  96.5 us (67%)
  matrix products  18.6 us (13%)
  starting transfers between devices  9.03 us (6%)
  local copies, waits for them, and re-layouts  7.4 us (5%)
  waiting for transfers between devices  6.66 us (5%)
  other arithmetic  3.44 us (2%)
  between operations  1.6 us (1%)
    unnamed x1, blocking collectives  94.6 us
    dot_general x1, matrix products, fold_accepted(): jnp.einsum('sph,sphd,sphv->shdv', weights, key_rows, value_rows, precisio...  7.97 us
    all_to_all x1, starting transfers between devices, shards(): lax.all_to_all(normed, 'kv', split_axis=1, concat_axis=0, tiled=True)  7.11 us
    unnamed x1, waiting for transfers between devices  6.66 us
    dot_general x1, matrix products, readout_block(): jnp.einsum('sthd,shdv->sthv', query_rows, base_mem, precision=highest)  4.24 us
  transfers between devices with their start and end apart: 2, of which 1 were waited for; matrix products, arithmetic and copies ran while one was open for 12% of the time, Pallas kernels for 0%

commit v1 on v0

--- a/solution.py
+++ b/solution.py
@@ -88,7 +88,15 @@
         * norm_gain
     ).astype(jnp.bfloat16)
     stacked = jnp.concatenate([w_query, w_key, w_value], axis=1)
-    spread = lax.all_to_all(normed, "kv", split_axis=1, concat_axis=0, tiled=True)
+    spread = jnp.concatenate(
+        jax.lax.all_to_all(
+            jnp.stack(jnp.split(normed, jax.lax.axis_size("kv"), axis=1)),
+            split_axis=0,
+            concat_axis=0,
+            axis_name="kv",
+        ),
+        axis=0,
+    )
     projected = lax.psum_scatter(
         jnp.dot(spread, stacked, preferred_element_type=jnp.float32),
         "kv",

time: 144 us -> 153 us (1.062)
  local copies, waits for them, and re-layouts: 7.4 us -> 16.3 us
    unnamed x22 -> x36, local copies, waits for them, and re-layouts: 1.8 us -> 10.7 us
  transfers between devices with their start and end apart: 2 -> 2, of which waited for: 1 -> 1; matrix products, arithmetic and copies ran while one was open for 12% -> 11% of each run, Pallas kernels for 0% -> 0%
where the time goes in v1:
time: 153 us; the launch traced here: 152 us
  blocking collectives  96.5 us (63%)
  matrix products  18.6 us (12%)
  local copies, waits for them, and re-layouts  16.3 us (11%)
  starting transfers between devices  9.03 us (6%)
  waiting for transfers between devices  6.65 us (4%)
  other arithmetic  3.44 us (2%)
  between operations  1.59 us (1%)
    unnamed x1, blocking collectives  94.6 us
    unnamed x36, local copies, waits for them, and re-layouts  10.7 us
    dot_general x1, matrix products, fold_accepted(): jnp.einsum('sph,sphd,sphv->shdv', weights, key_rows, value_rows, precisio...  7.96 us
    all_to_all x1, starting transfers between devices, shards(): jax.lax.all_to_all(jnp.stack(jnp.split(normed, jax.lax.axis_size('kv'), a...  7.11 us
    unnamed x1, waiting for transfers between devices  6.65 us
    dot_general x1, matrix products, readout_block(): jnp.einsum('sthd,shdv->sthv', query_rows, base_mem, precision=highest)  4.24 us
  transfers between devices with their start and end apart: 2, of which 1 were waited for; matrix products, arithmetic and copies ran while one was open for 11% of the time, Pallas kernels for 0%

profile of v1, /device:TPU:16, one launch (start us, length us, event | category | flops | bytes accessed | tf_op | source)
XLA Modules:
  0.0 152.0 jit_solution(486488416204563328)
XLA Ops:
  0.6 0.0 copy-start
  0.6 1.0 reshape.103
  1.6 1.9 %all_gather.3 = bf16[30,2048]{1,0:T(8,128)(2,1)S(1)} all-gather(bf16[30,1024]{1,0:T(8,128)(2,1)S(1)} %reshape.103), channel_id=1, replica_groups=mesh['kv'=16,'tp'=2] {'tp'}, dimensions={1}, use_global_device_ids=true | all-gather | bytes 184320 | tf_op jit(solution)/shard_map/all_gather | solution.py:83
  3.5 0.1 fusion.13
  3.7 0.8 fusion.15
  4.5 0.6 constant_dynamic-update-slice_fusion.15
  5.1 0.6 constant_dynamic-update-slice_fusion.14
  5.7 0.6 constant_dynamic-update-slice_fusion.13
  6.3 0.6 constant_dynamic-update-slice_fusion.12
  6.9 0.6 constant_dynamic-update-slice_fusion.11
  7.5 0.6 constant_dynamic-update-slice_fusion.10
  8.1 0.6 constant_dynamic-update-slice_fusion.9
  8.7 0.6 constant_dynamic-update-slice_fusion.8
  9.3 0.6 constant_dynamic-update-slice_fusion.7
  9.8 0.6 constant_dynamic-update-slice_fusion.6
  10.4 0.6 constant_dynamic-update-slice_fusion.5
  11.0 0.6 constant_dynamic-update-slice_fusion.4
  11.6 0.6 constant_dynamic-update-slice_fusion.3
  12.2 0.6 constant_dynamic-update-slice_fusion.2
  12.8 0.6 constant_dynamic-update-slice_fusion.1
  13.4 0.6 constant_dynamic-update-slice_fusion
  14.0 7.1 %all-to-all-start = ((bf16[16,30,128]{2,1,0:T(8,128)(2,1)}), bf16[16,30,128]{2,1,0:T(8,128)(2,1)S(1)}, u32[]{:S(2)}, u32[]{:S(2)}) async-start(bf16[16,30,128]{2,1,0:T(8,128)(2,1)} %constant_dynamic-update-slice_fusion), calls=%async_computation | async-start | bytes 262144 | tf_op jit(solution)/shard_map/all_to_all | solution.py:92
  21.2 0.7 iota_compare_fusion
  21.8 0.7 dynamic_slice.15
  22.6 0.7 dynamic_slice.13
  23.3 0.7 fusion.31
  24.0 0.1 copy.116
  24.1 0.7 fusion.44
  24.8 0.1 copy.138
  24.9 0.8 copy.117
  25.7 0.1 copy.119
  25.8 0.8 reshape.112
  26.6 0.9 fusion.37
  27.5 0.1 reshape.107
  27.6 0.1 copy.112
  27.7 0.1 copy.113
  27.8 0.9 convolution_add_fusion
  28.7 0.1 add.89
  28.9 0.2 fusion.19
  29.0 0.1 copy.120
  29.2 0.1 copy.125
  29.3 0.1 broadcast_multiply_fusion
  29.4 0.0 copy-start.7
  29.4 0.0 copy-start.2
  29.4 0.0 copy-start.3
  29.4 8.0 %multiply_add_fusion = f32[10,4,128,256]{3,2,1,0:T(8,128)} fusion(f32[10,4,128,256]{3,2,1,0:T(8,128)} %param.31, f32[10,4]{1,0:T(8,128)S(1)} %get-tuple-element.14, bf16[10,3,4,256]{3,1,2,0:T(4,128)(2,1)S(1)} %bitcast.117, f32[10,3,4,128]{3,2,1,0:T(4,128)S(1)} %get-tuple-element.19), kind=kOutput, calls=%fused_computation | convolution fusion | flops 49807360 | bytes 10608800 | tf_op jit(solution)/shard_map/sph,sphd,sphv->shdv/dot_general | solution.py:22
  37.4 0.1 copy.133
  37.5 0.1 copy.121
  37.6 0.6 dynamic-slice.4
  38.9 0.4 fusion.20
  39.4 2.5 %fusion.7 = f32[480,2048]{1,0:T(8,128)} fusion(bf16[480,128]{1,0:T(8,128)(2,1)S(1)} %reshape.104, bf16[128,1024]{1,0:T(8,128)(2,1)S(1)} %copy-done.1, bf16[128,512]{1,0:T(8,128)(2,1)S(1)} %copy-done.2, bf16[128,512]{1,0:T(8,128)(2,1)S(1)} %copy-done.3), kind=kOutput, calls=%fused_computation.12 | convolution fusion | flops 253231104 | bytes 4579328 | tf_op jit(solution)/shard_map/dot_general | solution.py:101
  41.9 94.6 %fusion = f32[32,2048]{1,0:T(8,128)S(1)} fusion(f32[480,2048]{1,0:T(8,128)} %fusion.7), kind=kCustom, calls=%all-reduce-scatter | all-reduce-scatter fusion | flops 1048577 | bytes 4194816
  136.6 1.9 %collective-permute-start = (bf16[30,2048]{1,0:T(8,128)(2,1)S(1)}, bf16[30,2048]{1,0:T(8,128)(2,1)S(1)}, u32[]{:S(2)}, u32[]{:S(2)}) collective-permute-start(bf16[30,2048]{1,0:T(8,128)(2,1)S(1)} %slice.23), channel_id=1, source_target_pairs={{0,2},{2,4},{4,6},{6,8},{8,10},{10,12},{12,14},{14,16},{16,18},{18... | collective-permute-start | bytes 368648
  138.5 0.1 multiply_add_fusion.1
  138.6 6.6 %collective-permute-done = bf16[30,2048]{1,0:T(8,128)(2,1)S(1)} collective-permute-done((bf16[30,2048]{1,0:T(8,128)(2,1)S(1)}, bf16[30,2048]{1,0:T(8,128)(2,1)S(1)}, u32[]{:S(2)}, u32[]{:S(2)}) %collective-permute-start) | collective-permute-done | bytes 122912
  145.3 0.3 concatenate.4
  145.6 0.3 fusion.23
  145.9 0.1 copy.137
  146.1 0.3 fusion.45
  146.4 0.1 copy.129
  146.6 0.1 copy.130
  146.7 0.1 copy.124
  146.8 4.2 %fusion.3 = f32[10,3,4,256]{3,1,2,0:T(4,128)S(1)} fusion(f32[10,4,128,256]{3,2,1,0:T(8,128)} %multiply_add_fusion, f32[10,3,4]{1,2,0:T(4,128)S(1)} %copy.124, bf16[10,3,4,128]{3,2,1,0:T(4,128)(2,1)S(1)} %reshape.106), kind=kOutput, calls=%fused_computation.5 | convolution fusion | flops 47216640 | bytes 5396960 | tf_op jit(solution)/shard_map/sthd,shdv->sthv/dot_general | solution.py:49
  151.0 1.0 fusion.4
  (30 shorter events, 0.3 us)
Async XLA Ops:
  0.6 28.8 %copy-start = (bf16[10,3,1024]{2,1,0:T(4,128)(2,1)S(1)}, bf16[10,3,1024]{2,1,0:T(4,128)(2,1)}, u32[]{:S(2)}) copy-start(bf16[10,3,1024]{2,1,0:T(4,128)(2,1)} %param.27) | copy-start | bytes 184324
  14.0 25.2 %all-to-all-start = ((bf16[16,30,128]{2,1,0:T(8,128)(2,1)}), bf16[16,30,128]{2,1,0:T(8,128)(2,1)S(1)}, u32[]{:S(2)}, u32[]{:S(2)}) async-start(bf16[16,30,128]{2,1,0:T(8,128)(2,1)} %constant_dynamic-update-slice_fusion), calls=%async_computation | async-start | bytes 262144 | tf_op jit(solution)/shard_map/all_to_all | solution.py:92
  25.8 120.8 %copy-start.6 = (f32[10,4]{0,1:T(4,128)}, f32[10,4]{0,1:T(4,128)S(1)}, u32[]{:S(2)}) copy-start(f32[10,4]{0,1:T(4,128)S(1)} %copy.119) | copy-start | bytes 484
  29.4 8.2 %copy-start.7 = (u32[32]{0:T(128)S(1)}, u32[32]{0:T(128)}, u32[]{:S(2)}) copy-start(u32[32]{0:T(128)} %constant.39) | copy-start | bytes 388
  29.4 9.9 %copy-start.1 = (bf16[128,1024]{1,0:T(8,128)(2,1)S(1)}, bf16[128,1024]{1,0:T(8,128)(2,1)}, u32[]{:S(2)}) copy-start(bf16[128,1024]{1,0:T(8,128)(2,1)} %param.21) | copy-start | bytes 786436
  29.4 9.9 %copy-start.2 = (bf16[128,512]{1,0:T(8,128)(2,1)S(1)}, bf16[128,512]{1,0:T(8,128)(2,1)}, u32[]{:S(2)}) copy-start(bf16[128,512]{1,0:T(8,128)(2,1)} %param.20) | copy-start | bytes 393220
  29.4 9.9 %copy-start.3 = (bf16[128,512]{1,0:T(8,128)(2,1)S(1)}, bf16[128,512]{1,0:T(8,128)(2,1)}, u32[]{:S(2)}) copy-start(bf16[128,512]{1,0:T(8,128)(2,1)} %param.19) | copy-start | bytes 393220
  39.4 99.2 %copy-start.4 = (f32[10,4,128]{2,1,0:T(4,128)S(1)}, f32[10,4,128]{2,1,0:T(4,128)}, u32[]{:S(2)}) copy-start(f32[10,4,128]{2,1,0:T(4,128)} %param.32) | copy-start | bytes 61444
  136.6 8.7 %collective-permute-start = (bf16[30,2048]{1,0:T(8,128)(2,1)S(1)}, bf16[30,2048]{1,0:T(8,128)(2,1)S(1)}, u32[]{:S(2)}, u32[]{:S(2)}) collective-permute-start(bf16[30,2048]{1,0:T(8,128)(2,1)S(1)} %slice.23), channel_id=1, source_target_pairs={{0,2},{2,4},{4,6},{6,8},{8,10},{10,12},{12,14},{14,16},{16,18},{18... | collective-permute-start | bytes 368648
  138.6 13.4 %copy-start.5 = (f32[10,4,128]{2,1,0:T(4,128)}, f32[10,4,128]{2,1,0:T(4,128)S(1)}, u32[]{:S(2)}) copy-start(f32[10,4,128]{2,1,0:T(4,128)S(1)} %multiply_add_fusion.1) | copy-start | bytes 61444
